TPU v7x, 512 devices: a 4x2x32 block of a 4x8x32 slice. The times are simulated.
512 devices in a mesh: grp: 2 (over y), fs: 32 (over z), tp: 8 (over x, core).
Axes of the slice: x: 4, y: 2, z: 32, core: 2. Of those that a mesh axis runs over, the one named last changes fastest.
The devices are a block of a 4x8x32 slice.
Arguments:
- tokens: bfloat16 [32768, 2048], P(('grp', 'fs')), parts along dimension 0, may hold values from -6 to 6
- pre_gain: float32 [2048], replicated, may hold values from 0.1 to 1.9
- up_weight: float32 [2048, 8192], P('fs', 'tp'), may hold values from -0.125 to 0.125
- up_scale: float32 [8192], P('tp'), may hold values from 0.3 to 3
- down_weight: float32 [8192, 2048], P('tp', 'fs'), may hold values from -0.0625 to 0.0625
- down_scale: float32 [2048], P('fs'), may hold values from 0.3 to 3
- post_gain: float32 [2048], replicated, may hold values from 0.1 to 1.9
Outputs:
- mixed: bfloat16 [32768, 2048], P(('grp', 'fs')), parts along dimension 0
There are 2 independent parts, one for each index of `grp`. A program takes and returns all parts, laid end to end along the dimension named above; an argument that names none is the same for every part. Nothing has to cross between parts.
All inputs are finite; a program needn't handle non-finite values.
Results may differ from a plain program's by a relative error of at most 0.01.
Values may be sent and summed in bfloat16 or wider, within the bound.
A program may use at most 64 MiB of HBM per device.

v0:
```python
import jax
import jax.numpy as jnp
from jax import lax
from jax.sharding import PartitionSpec as P

epsilon = 1e-06


def joined_along(parts, dim):
    shape = list(parts.shape[1:])
    shape[dim] *= parts.shape[0]
    return jnp.moveaxis(parts, 0, dim).reshape(shape)


def sent_to_all(shard, axis):
    length = lax.axis_size(axis)
    return lax.all_to_all(
        jnp.broadcast_to(shard[None], (length, *shard.shape)), axis, 0, 0, tiled=True
    )


def gathered_copies(shard, axis, dim):
    return joined_along(sent_to_all(shard, axis), dim)


def turned_gather(arrays, axis, dims):
    turned = [jnp.moveaxis(a, dim, 0) for a, dim in zip(arrays, dims)]
    widths = [t[0].size for t in turned]
    both = jnp.concatenate([t.reshape(-1, w) for t, w in zip(turned, widths)], axis=1)
    whole = lax.all_gather(both, axis, axis=0, tiled=True)
    parts = jnp.split(whole, [sum(widths[:k]) for k in range(1, len(widths))], axis=1)
    return tuple(
        (
            jnp.moveaxis(b.reshape(-1, *t.shape[1:]), 0, dim)
            for b, t, dim in zip(parts, turned, dims)
        )
    )


def in_blocks(shard, dim, length):
    before, after = (shard.shape[:dim], shard.shape[dim + 1 :])
    return jnp.moveaxis(shard.reshape(*before, length, -1, *after), dim, 0)


def summed_on_arrival(shard, axis, dim):
    parts = in_blocks(shard, dim, lax.axis_size(axis))
    arrived = lax.all_to_all(parts, axis, split_axis=0, concat_axis=0, tiled=True)
    return arrived.astype(jnp.float32).sum(axis=0)


def rms_rows(values, scaling):
    return values * lax.rsqrt(jnp.mean(values * values, axis=-1, keepdims=True) + epsilon) * scaling


def activate(lifted, up_scale):
    return jnp.square(jax.nn.relu(lifted * up_scale)).astype(jnp.bfloat16)


def on_device(tokens, pre_gain, up_weight, up_scale, down_weight, down_scale, post_gain):
    residual = tokens.astype(jnp.float32)
    normed = rms_rows(residual, pre_gain).astype(jnp.bfloat16)
    up_cast = up_weight.astype(jnp.bfloat16)
    down_cast = down_weight.astype(jnp.bfloat16)
    column_scales = gathered_copies(down_scale, "fs", 0)
    up_full, down_full = turned_gather((up_cast, down_cast), "fs", (0, 1))
    lifted = jnp.dot(normed, up_full, preferred_element_type=jnp.float32)
    hidden = activate(lifted, up_scale)
    partials = jnp.dot(hidden, down_full, preferred_element_type=jnp.float32)
    partials = (partials * column_scales).astype(jnp.bfloat16)
    summed = summed_on_arrival(partials, "tp", 0)
    branch = lax.optimization_barrier(summed.astype(jnp.bfloat16)).astype(jnp.float32)
    row_count = branch.shape[0]
    offset = lax.axis_index("tp") * row_count
    own_rows = lax.dynamic_slice_in_dim(residual, offset, row_count, 0)
    result = (own_rows + rms_rows(branch, post_gain)).astype(jnp.bfloat16)
    return gathered_copies(result, "tp", 0)


def solution(mesh):
    placed = (P(("grp", "fs"), None), P(), P("fs", "tp"), P("tp"), P("tp", "fs"), P("fs"), P())
    return jax.shard_map(
        on_device, mesh=mesh, in_specs=placed, out_specs=P(("grp", "fs"), None), check_vma=False
    )
```

profile of v0, /device:TPU:33, one launch (start us, length us, event | category | flops | bytes accessed | tf_op | source)
XLA Modules:
  0.0 268.8 jit_solution(17365989303714553077)
XLA Ops:
  6.5 0.0 all-gather.2.cloned.1.call-start
  6.6 1.0 convert_bitcast_fusion
  7.5 1.0 convert_element_type.28
  8.5 0.7 pad_maximum_fusion
  9.2 0.1 all-gather.2.cloned.1.call-update
  9.3 1.3 broadcast_in_dim.4
  10.5 46.3 %all-to-all-start = ((f32[32,1,64]{2,1,0:T(1,128)}), f32[32,1,64]{2,1,0:T(1,128)S(1)}, u32[]{:S(2)}, u32[]{:S(2)}) async-start(f32[32,1,64]{2,1,0:T(1,128)} %broadcast_in_dim.4), calls=%async_computation | async-start | bytes 32768 | tf_op jit(solution)/shard_map/all_to_all | solution.py:17
  56.8 2.1 multiply_reduce_fusion
  58.9 18.4 %all-to-all-done = f32[32,1,64]{2,1,0:T(1,128)S(1)} async-done(((f32[32,1,64]{2,1,0:T(1,128)}), f32[32,1,64]{2,1,0:T(1,128)S(1)}, u32[]{:S(2)}, u32[]{:S(2)}) %all-to-all-start) | async-done | bytes 8224 | tf_op jit(solution)/shard_map/all_to_all | solution.py:17
  77.4 0.5 broadcast.32
  77.9 0.6 reduce.4
  78.5 0.1 mul.67
  78.5 88.1 %all-gather.2.cloned.1.call-done = bf16[2048,2048]{1,0:T(8,128)(2,1)} async-done(((bf16[64,2048]{1,0:T(8,128)(2,1)}), bf16[2048,2048]{1,0:T(8,128)(2,1)}) %all-gather.2.cloned.1.call-update) | async-done | bytes 8388624 | tf_op jit(solution)/shard_map/all_gather | solution.py:30
  166.6 9.9 %multiply_convert_fusion = bf16[512,2048]{1,0:T(8,128)(2,1)} fusion(bf16[2048,2048]{1,0:T(8,128)(2,1)} %all-gather.2.cloned.1.call-done, f32[2048]{0:T(1024)S(1)} %mul.67, f32[2048]{0:T(1024)} %param.8, f32[512]{0:T(512)S(1)} %add_rsqrt_fusion, bf16[512,2048]{1,0:T(8,128)(2,1)} %param.7, f32[1024]{0:T(1024)} %param.10), kind=kOutput, calls=%fused_computation.4 | convolution fusion | flops 4303355904 | bytes 12605440 | tf_op jit(solution)/shard_map/dot_general | solution.py:68
  176.6 0.0 copy-start
  176.6 24.5 %all-to-all-start.1 = ((bf16[8,64,2048]{2,1,0:T(8,128)(2,1)}), bf16[8,64,2048]{2,1,0:T(8,128)(2,1)}, u32[]{:S(2)}, u32[]{:S(2)}) async-start(bf16[8,64,2048]{2,1,0:T(8,128)(2,1)} %bitcast.5), calls=%async_computation.1 | async-start | bytes 4194304 | tf_op jit(solution)/shard_map/all_to_all | solution.py:47
  201.1 0.0 copy-done
  201.1 0.0 copy-start.1
  201.1 2.5 convert_element_type.26
  203.5 23.9 %all-to-all-done.1 = bf16[8,64,2048]{2,1,0:T(8,128)(2,1)} async-done(((bf16[8,64,2048]{2,1,0:T(8,128)(2,1)}), bf16[8,64,2048]{2,1,0:T(8,128)(2,1)}, u32[]{:S(2)}, u32[]{:S(2)}) %all-to-all-start.1) | async-done | bytes 2097184 | tf_op jit(solution)/shard_map/all_to_all | solution.py:47
  227.4 2.0 reduce_sum.31
  229.3 0.2 fusion.15
  229.5 0.0 copy-done.1
  229.5 1.2 fusion.18
  230.7 0.2 broadcast_in_dim.5
  231.0 29.7 %all_to_all.16 = bf16[8,64,2048]{2,1,0:T(8,128)(2,1)S(1)} all-to-all(bf16[8,64,2048]{2,1,0:T(8,128)(2,1)S(1)} %broadcast_in_dim.5), channel_id=1, replica_groups=mesh['grp'=2,'fs'=32,'tp'=8] {'tp'}, dimensions={0} | all-to-all | bytes 4194304 | tf_op jit(solution)/shard_map/all_to_all | solution.py:17
  260.6 1.3 copy.9
  (2 shorter events, 0.0 us)
Async XLA Ops:
  6.5 160.1 %all-gather.2.cloned.1.call-start = ((), (), s32[]{:S(2)}) async-start(), calls=%async_computation.3 | async-start | bytes 8650752 | tf_op jit(solution)/shard_map/all_gather | solution.py:30
  10.5 66.8 %all-to-all-start = ((f32[32,1,64]{2,1,0:T(1,128)}), f32[32,1,64]{2,1,0:T(1,128)S(1)}, u32[]{:S(2)}, u32[]{:S(2)}) async-start(f32[32,1,64]{2,1,0:T(1,128)} %broadcast_in_dim.4), calls=%async_computation | async-start | bytes 32768 | tf_op jit(solution)/shard_map/all_to_all | solution.py:17
  176.6 24.5 %copy-start = (bf16[512,2048]{1,0:T(8,128)(2,1)S(1)}, bf16[512,2048]{1,0:T(8,128)(2,1)}, u32[]{:S(2)}) copy-start(bf16[512,2048]{1,0:T(8,128)(2,1)} %param.7) | copy-start | bytes 6291460
  176.6 50.8 %all-to-all-start.1 = ((bf16[8,64,2048]{2,1,0:T(8,128)(2,1)}), bf16[8,64,2048]{2,1,0:T(8,128)(2,1)}, u32[]{:S(2)}, u32[]{:S(2)}) async-start(bf16[8,64,2048]{2,1,0:T(8,128)(2,1)} %bitcast.5), calls=%async_computation.1 | async-start | bytes 4194304 | tf_op jit(solution)/shard_map/all_to_all | solution.py:47
  201.1 28.4 %copy-start.1 = (f32[2048]{0:T(1024)S(1)}, f32[2048]{0:T(1024)}, u32[]{:S(2)}) copy-start(f32[2048]{0:T(1024)} %param.13) | copy-start | bytes 24580
Sparse Core Ops, SparseCore 0:
  9.4 157.1 all-gather.1
where the time goes:
time: 269 us
  waiting for transfers between devices  130 us (48%)
  starting transfers between devices  70.8 us (26%)
  blocking collectives  29.7 us (11%)
  between operations  13.5 us (5%)
  other arithmetic  11.1 us (4%)
  matrix products  9.94 us (4%)
  local copies, waits for them, and re-layouts  3.39 us (1%)
    all_gather x1, waiting for transfers between devices, turned_gather(): whole = lax.all_gather(both, axis, axis=0, tiled=True)  88.1 us
    all_to_all x1, starting transfers between devices, sent_to_all(): lax.all_to_all(jnp.broadcast_to(shard[None], (length, *shard.shape)), axi...  46.3 us
    all_to_all x1, blocking collectives, sent_to_all(): lax.all_to_all(jnp.broadcast_to(shard[None], (length, *shard.shape)), axi...  29.7 us
    all_to_all x1, starting transfers between devices, summed_on_arrival(): lax.all_to_all(parts, axis, split_axis=0, concat_axis=0, tiled=True)  24.5 us
    all_to_all x1, waiting for transfers between devices, summed_on_arrival(): lax.all_to_all(parts, axis, split_axis=0, concat_axis=0, tiled=True)  23.9 us
    all_to_all x1, waiting for transfers between devices, sent_to_all(): lax.all_to_all(jnp.broadcast_to(shard[None], (length, *shard.shape)), axi...  18.4 us
    dot_general x1, matrix products, on_device(): partials = jnp.dot(hidden, down_full, preferred_element_type=jnp.float32)  9.94 us
  transfers between devices with their start and end apart: 3, of which 3 were waited for; matrix products, arithmetic and copies ran while one was open for 3% of the time, Pallas kernels for 0%

commit v1 on v0

--- a/solution.py
+++ b/solution.py
@@ -27,7 +27,9 @@
     turned = [jnp.moveaxis(a, dim, 0) for a, dim in zip(arrays, dims)]
     widths = [t[0].size for t in turned]
     both = jnp.concatenate([t.reshape(-1, w) for t, w in zip(turned, widths)], axis=1)
-    whole = lax.all_gather(both, axis, axis=0, tiled=True)
+    whole = jnp.concatenate(
+        lax.all_to_all(jnp.stack([both] * lax.axis_size(axis)), axis, 0, 0), axis=0
+    )
     parts = jnp.split(whole, [sum(widths[:k]) for k in range(1, len(widths))], axis=1)
     return tuple(
         (

time: 269 us -> 886 us (3.29)
  the two profiles are of different devices: /device:TPU:33 before, /device:TPU:224 now
where the time goes in v1:
time: 886 us
  waiting for transfers between devices  775 us (87%)
  starting transfers between devices  54.5 us (6%)
  blocking collectives  29.7 us (3%)
  matrix products  9.35 us (1%)
  other arithmetic  8.91 us (1%)
    all_to_all x1, waiting for transfers between devices, turned_gather(): lax.all_to_all(jnp.stack([both] * lax.axis_size(axis)), axis, 0, 0)  733 us
    all_to_all x1, starting transfers between devices, sent_to_all(): lax.all_to_all(jnp.broadcast_to(shard[None], (length, *shard.shape)), axi...  41.7 us
    all_to_all x1, blocking collectives, sent_to_all(): lax.all_to_all(jnp.broadcast_to(shard[None], (length, *shard.shape)), axi...  29.7 us
    all_to_all x1, waiting for transfers between devices, summed_on_arrival(): lax.all_to_all(parts, axis, split_axis=0, concat_axis=0, tiled=True)  24.8 us
  transfers between devices with their start and end apart: 3, of which 3 were waited for; matrix products, arithmetic and copies ran while one was open for 1% of the time, Pallas kernels for 0%

profile of v1, /device:TPU:224, one launch (start us, length us, event | category | flops | bytes accessed | tf_op | source)
XLA Modules:
  0.0 885.5 jit_solution(14603014351865717425)
XLA Ops:
  0.0 1.3 broadcast_in_dim.4
  1.3 41.7 %all-to-all-start.1 = ((f32[32,1,64]{2,1,0:T(1,128)}), f32[32,1,64]{2,1,0:T(1,128)S(1)}, u32[]{:S(2)}, u32[]{:S(2)}) async-start(f32[32,1,64]{2,1,0:T(1,128)} %broadcast_in_dim.4), calls=%async_computation.1 | async-start | bytes 32768 | tf_op jit(solution)/shard_map/all_to_all | solution.py:17
  43.0 1.0 convert_bitcast_fusion
  43.9 1.0 convert_element_type.28
  44.9 17.0 %all-to-all-done.1 = f32[32,1,64]{2,1,0:T(1,128)S(1)} async-done(((f32[32,1,64]{2,1,0:T(1,128)}), f32[32,1,64]{2,1,0:T(1,128)S(1)}, u32[]{:S(2)}, u32[]{:S(2)}) %all-to-all-start.1) | async-done | bytes 8224 | tf_op jit(solution)/shard_map/all_to_all | solution.py:17
  62.0 4.3 stack.2
  66.2 0.0 copy-start
  66.2 0.0 copy-start.2
  66.3 0.0 copy-start.3
  66.3 8.2 all-to-all-start
  74.5 0.0 copy-done
  74.5 0.5 multiply_reduce_fusion
  75.0 0.5 broadcast.34
  75.5 0.7 reduce.4
  76.2 0.1 mul.67
  76.2 733.4 %all-to-all-done = bf16[32,64,2048]{2,1,0:T(8,128)(2,1)} async-done(((bf16[32,64,2048]{2,1,0:T(8,128)(2,1)}), bf16[32,64,2048]{2,1,0:T(8,128)(2,1)}, u32[]{:S(2)}, u32[]{:S(2)}) %all-to-all-start) | async-done | bytes 8388640 | tf_op jit(solution)/shard_map/all_to_all | solution.py:31
  809.7 0.0 copy-done.2
  809.7 0.0 copy-done.3
  809.7 9.4 %multiply_convert_fusion = bf16[512,2048]{1,0:T(8,128)(2,1)} fusion(bf16[2048,2048]{1,0:T(8,128)(2,1)} %bitcast.1, f32[2048]{0:T(1024)S(1)} %mul.67, f32[2048]{0:T(1024)S(1)} %copy-done.2, f32[512]{0:T(512)S(1)} %add_rsqrt_fusion, bf16[512,2048]{1,0:T(8,128)(2,1)S(1)} %copy-done, f32[1024]{0:T(1024)S(1)} %copy-done.3), kind=kOutput, calls=%fused_computation.4 | convolution fusion | flops 4303355904 | bytes 12605440 | tf_op jit(solution)/shard_map/dot_general | solution.py:70
  819.0 4.6 all-to-all-start.2
  823.6 0.0 copy-start.1
  823.6 2.5 convert_element_type.26
  826.1 24.8 %all-to-all-done.2 = bf16[8,64,2048]{2,1,0:T(8,128)(2,1)} async-done(((bf16[8,64,2048]{2,1,0:T(8,128)(2,1)}), bf16[8,64,2048]{2,1,0:T(8,128)(2,1)}, u32[]{:S(2)}, u32[]{:S(2)}) %all-to-all-start.2) | async-done | bytes 2097184 | tf_op jit(solution)/shard_map/all_to_all | solution.py:49
  850.9 2.0 reduce_sum.31
  852.9 0.2 fusion.15
  853.0 0.0 copy-done.1
  853.0 1.2 fusion.18
  854.2 0.2 broadcast_in_dim.5
  854.5 29.7 %all_to_all.21 = bf16[8,64,2048]{2,1,0:T(8,128)(2,1)S(1)} all-to-all(bf16[8,64,2048]{2,1,0:T(8,128)(2,1)S(1)} %broadcast_in_dim.5), channel_id=1, replica_groups=mesh['grp'=2,'fs'=32,'tp'=8] {'tp'}, dimensions={0} | all-to-all | bytes 4194304 | tf_op jit(solution)/shard_map/all_to_all | solution.py:17
  884.2 1.3 copy.9
  (3 shorter events, 0.0 us)
Async XLA Ops:
  1.3 60.7 %all-to-all-start.1 = ((f32[32,1,64]{2,1,0:T(1,128)}), f32[32,1,64]{2,1,0:T(1,128)S(1)}, u32[]{:S(2)}, u32[]{:S(2)}) async-start(f32[32,1,64]{2,1,0:T(1,128)} %broadcast_in_dim.4), calls=%async_computation.1 | async-start | bytes 32768 | tf_op jit(solution)/shard_map/all_to_all | solution.py:17
  66.2 8.2 copy-start
  66.2 743.4 %copy-start.2 = (f32[2048]{0:T(1024)S(1)}, f32[2048]{0:T(1024)}, u32[]{:S(2)}) copy-start(f32[2048]{0:T(1024)} %param.8) | copy-start | bytes 24580
  66.3 743.4 %copy-start.3 = (f32[1024]{0:T(1024)S(1)}, f32[1024]{0:T(1024)}, u32[]{:S(2)}) copy-start(f32[1024]{0:T(1024)} %param.10) | copy-start | bytes 12292
  66.3 743.4 %all-to-all-start = ((bf16[32,64,2048]{2,1,0:T(8,128)(2,1)}), bf16[32,64,2048]{2,1,0:T(8,128)(2,1)}, u32[]{:S(2)}, u32[]{:S(2)}) async-start(bf16[32,64,2048]{2,1,0:T(8,128)(2,1)} %stack.2), calls=%async_computation | async-start | bytes 16777216 | tf_op jit(solution)/shard_map/all_to_all | solution.py:31
  819.0 31.9 %all-to-all-start.2 = ((bf16[8,64,2048]{2,1,0:T(8,128)(2,1)}), bf16[8,64,2048]{2,1,0:T(8,128)(2,1)}, u32[]{:S(2)}, u32[]{:S(2)}) async-start(bf16[8,64,2048]{2,1,0:T(8,128)(2,1)} %bitcast.6), calls=%async_computation.2 | async-start | bytes 4194304 | tf_op jit(solution)/shard_map/all_to_all | solution.py:49
  823.6 29.4 %copy-start.1 = (f32[2048]{0:T(1024)S(1)}, f32[2048]{0:T(1024)}, u32[]{:S(2)}) copy-start(f32[2048]{0:T(1024)} %param.13) | copy-start | bytes 24580
